TPU v7x, 32 devices: a whole 2x2x4 slice. The times are simulated.
32 devices in a mesh: rep: 2 (over x), fs: 8 (over z, y), tp: 2 (over core).
Axes of the slice: x: 2, y: 2, z: 4, core: 2. Of those that a mesh axis runs over, the one named last changes fastest.
Arguments:
- inputs: bfloat16 [2, 3072, 2048], P('rep', 'fs', 'tp'), may hold values from -6 to 6
- gate_proj: bfloat16 [2048, 2816], P('fs', 'tp'), may hold values from -0.125 to 0.125
- value_proj: bfloat16 [2048, 2816], P('fs', 'tp'), may hold values from -0.125 to 0.125
- gate_taps: float32 [3, 2816], replicated, may hold values from -3 to 3
- value_taps: float32 [3, 2816], replicated, may hold values from -3 to 3
- out_grad: bfloat16 [2, 3072, 2816], P('rep', 'fs', 'tp'), may hold values from -6 to 6
Outputs:
- in_grad: bfloat16 [2, 3072, 2048], P('rep', 'fs', 'tp')
- gate_proj_grad: float32 [2048, 2816], P('fs', 'tp')
- value_proj_grad: float32 [2048, 2816], P('fs', 'tp')
- gate_taps_grad: float32 [3, 2816], replicated
- value_taps_grad: float32 [3, 2816], replicated
All inputs are finite; a program needn't handle non-finite values.
Results may differ from a plain program's by a relative error of at most 0.013.
Values may be sent and summed in bfloat16 or wider, within the bound.
A program may use at most 128 MiB of HBM per device.

v0:
```python
import jax
import jax.numpy as jnp
from jax import lax
from jax.sharding import PartitionSpec as P


def with_halo(cells, sides, width):
    for axis, dim in sides:
        count = lax.axis_size(axis)
        ends = count - 1
        head = lax.slice_in_dim(cells, 0, width, axis=dim)
        tail = lax.slice_in_dim(cells, cells.shape[dim] - width, cells.shape[dim], axis=dim)
        cells = jnp.concatenate(
            [
                lax.ppermute(tail, axis, [(i, (i + 1) % count) for i in range(ends)]),
                cells,
                lax.ppermute(head, axis, [((i + 1) % count, i) for i in range(ends)]),
            ],
            axis=dim,
        )
    return cells


def mix_taps(pre_wide, taps_both, count):
    return (
        taps_both[:, 0, None, :] * pre_wide[:, 0:count]
        + taps_both[:, 1, None, :] * pre_wide[:, 1 : count + 1]
        + taps_both[:, 2, None, :] * pre_wide[:, 2 : count + 2]
    )


def back_taps(cot_wide, taps_both, count):
    return (
        taps_both[:, 0, None, :] * cot_wide[:, 2 : count + 2]
        + taps_both[:, 1, None, :] * cot_wide[:, 1 : count + 1]
        + taps_both[:, 2, None, :] * cot_wide[:, 0:count]
    )


def cotangents(gate_mix, value_mix, cot_in):
    sigmoid_gate = jax.nn.sigmoid(gate_mix)
    gate_cot = cot_in * value_mix * (sigmoid_gate * (1.0 + gate_mix * (1.0 - sigmoid_gate)))
    value_cot = cot_in * (gate_mix * sigmoid_gate)
    return (gate_cot, value_cot)


def shards(inputs, gate_proj, value_proj, gate_taps, value_taps, out_grad):
    contract_cols = (((1,), (1,)), ((), ()))
    contract_rows = (((0,), (0,)), ((), ()))
    tok_rows = inputs.shape[1]
    hid_cols = gate_proj.shape[1]
    gathered = lax.all_gather(inputs, "tp", axis=2, tiled=True)[0]
    col_start = lax.axis_index("tp") * hid_cols
    taps_both = jnp.stack(
        [
            lax.dynamic_slice_in_dim(gate_taps, col_start, hid_cols, 1),
            lax.dynamic_slice_in_dim(value_taps, col_start, hid_cols, 1),
        ]
    )
    stacked = jnp.stack([gate_proj, value_proj])
    full_rows = lax.all_gather(stacked, "fs", axis=1, tiled=True)
    gate_acc = jnp.dot(gathered, full_rows[0], preferred_element_type=jnp.float32)
    value_acc = jnp.dot(gathered, full_rows[1], preferred_element_type=jnp.float32)
    pre_acts = jnp.stack([gate_acc, value_acc]).astype(jnp.bfloat16)
    pre_wide = with_halo(pre_acts, (("fs", 1),), 1).astype(jnp.float32)
    mix_out = mix_taps(pre_wide, taps_both, tok_rows)
    gate_cot, value_cot = cotangents(mix_out[0], mix_out[1], out_grad[0].astype(jnp.float32))
    cot_rows = jnp.stack([gate_cot, value_cot])
    cot_wide = with_halo(cot_rows, (("fs", 1),), 1)
    pre_cot = back_taps(cot_wide, taps_both, tok_rows).astype(jnp.bfloat16)
    tap_terms = jnp.stack(
        [
            jnp.sum(pre_wide[:, offset : offset + tok_rows] * cot_rows, axis=1)
            for offset in range(3)
        ],
        axis=1,
    )
    partial_value = lax.dot_general(
        pre_cot[0], full_rows[0], contract_cols, preferred_element_type=jnp.float32
    ) + lax.dot_general(pre_cot[1], full_rows[1], contract_cols, preferred_element_type=jnp.float32)
    in_grad = lax.psum_scatter(
        partial_value.astype(jnp.bfloat16), "tp", scatter_dimension=1, tiled=True
    )[None]
    grad_terms = jnp.stack(
        [
            lax.dot_general(
                gathered, pre_cot[0], contract_rows, preferred_element_type=jnp.float32
            ),
            lax.dot_general(
                gathered, pre_cot[1], contract_rows, preferred_element_type=jnp.float32
            ),
        ]
    )
    received = lax.all_to_all(grad_terms, "fs", split_axis=1, concat_axis=0, tiled=True)
    fs_count = lax.axis_size("fs")
    own_sum = jnp.sum(received.reshape(fs_count, 2, received.shape[1], hid_cols), axis=0)
    own_sum = lax.psum(own_sum, "rep")
    taps_total = lax.psum(tap_terms, ("rep", "fs"))
    taps_all = lax.all_gather(taps_total, "tp", axis=2, tiled=True)
    factor = float(tok_rows * fs_count * lax.axis_size("rep")) ** (-0.5)
    return (
        in_grad,
        own_sum[0] * factor,
        own_sum[1] * factor,
        taps_all[0] * factor,
        taps_all[1] * factor,
    )


def solution(mesh):
    placed = (P("rep", "fs", "tp"), P("fs", "tp"), P("fs", "tp"), P(), P(), P("rep", "fs", "tp"))
    return jax.shard_map(
        shards,
        mesh=mesh,
        in_specs=placed,
        out_specs=(P("rep", "fs", "tp"), P("fs", "tp"), P("fs", "tp"), P(), P()),
        check_vma=False,
    )
```

profile of v0, /device:TPU:0, one launch (start us, length us, event | category | flops | bytes accessed | tf_op | source)
XLA Modules:
  0.0 895.8 jit_solution(16382616148427703612)
XLA Ops:
  7.2 0.0 copy-start.3
  7.2 0.0 copy-start.4
  7.2 0.0 all-gather.5.cloned.1.call-start
  7.2 0.7 all-gather.5.cloned.1.call-update
  7.9 0.0 all-gather.3.cloned.1.call-start
  8.0 2.6 pad_maximum_fusion.6
  10.5 0.0 all-gather.3.cloned.1.call-update
  10.6 0.0 all-reduce.2.cloned.1.call-start
  10.6 0.0 copy-done.3
  10.6 0.0 copy-done.4
  10.7 11.4 %all-gather.5.cloned.1.call-done = bf16[1,384,2048]{2,1,0:T(8,128)(2,1)} async-done(((bf16[1,384,1024]{2,1,0:T(8,128)(2,1)}), bf16[1,384,2048]{2,1,0:T(8,128)(2,1)}) %all-gather.5.cloned.1.call-update) | async-done | bytes 1572880 | tf_op jit(solution)/shard_map/all_gather | solution.py:52
  22.1 0.0 copy-start.6
  22.1 167.3 %all-gather.3.cloned.1.call-done = bf16[2,2048,1408]{2,1,0:T(8,128)(2,1)} async-done(((bf16[2,256,1408]{2,1,0:T(8,128)(2,1)}), bf16[2,2048,1408]{2,1,0:T(8,128)(2,1)}) %all-gather.3.cloned.1.call-update) | async-done | bytes 11534352 | tf_op jit(solution)/shard_map/all_gather | solution.py:61
  189.4 0.0 copy-start.5
  189.4 5.8 fusion.12
  195.2 0.0 copy-done.6
  195.2 0.5 copy-done.5
  195.8 2.6 fusion.11
  198.4 1.3 collective-permute-start.1
  199.7 4.5 collective-permute-start
  204.3 0.0 collective-permute-done.1
  204.3 1.3 collective-permute-done
  205.7 0.5 maximum_convert_fusion
  206.1 0.0 copy-start.2
  206.1 1.3 multiply_add_fusion
  207.4 0.0 copy-done.2
  207.4 1.2 convert_multiply_fusion
  208.6 4.2 collective-permute-start.3
  212.8 1.5 collective-permute-start.2
  214.3 0.0 collective-permute-done.3
  214.3 4.4 collective-permute-done.2
  218.7 4.2 multiply_reduce_fusion.2
  222.9 0.0 copy-start
  222.9 3.2 convolution_bitcast_fusion
  226.1 0.0 copy-done
  226.1 3.2 convolution_bitcast_fusion.1
  229.3 8.8 pad_maximum_fusion
  238.1 34.1 %copy.11 = f32[2,2048,1408]{2,0,1:T(2,128)} copy(f32[2,2048,1408]{1,2,0:T(8,128)} %pad_maximum_fusion) | data formatting | bytes 46137344 | tf_op jit(solution)/shard_map/stack | solution.py:84
  272.2 503.7 %all_to_all.12 = f32[2,2048,1408]{2,0,1:T(2,128)} all-to-all(f32[2,2048,1408]{2,0,1:T(2,128)} %copy.11), channel_id=1, replica_groups=mesh['rep'=2,'fs'=8,'tp'=2] {'fs'}, dimensions={1} | all-to-all | bytes 46137344 | tf_op jit(solution)/shard_map/all_to_all | solution.py:94
  775.9 10.5 %reduce_sum.36 = f32[2,256,1408]{2,0,1:T(2,128)S(1)} reduce(f32[2,8,256,1408]{3,0,2,1:T(2,128)} %bitcast.69, f32[]{:T(128)} %constant.4.clone.1), dimensions={1}, to_apply=%region_1.0 | reduce | flops 5046272 | bytes 25952260 | tf_op jit(solution)/shard_map/reduce_sum | solution.py:96
  786.4 3.8 copy.15
  790.2 0.0 all-reduce.2.cloned.1.call-update
  790.2 0.0 copy-start.1
  790.2 0.3 reduce-scatter.2.cloned.1.call-start
  790.5 5.1 fusion.2
  795.6 0.0 copy-done.1
  795.6 8.2 add_convert_fusion
  803.9 0.0 reduce-scatter.2.cloned.1.call-update
  804.0 77.6 %psum.15 = f32[2,3,1408]{2,1,0:T(4,128)S(1)} all-reduce(f32[2,3,1408]{2,1,0:T(4,128)S(1)} %pad_maximum_fusion.7), channel_id=1, replica_groups=mesh['rep'=2,'fs'=8,'tp'=2] {'rep','fs'}, use_global_device_ids=true, to_apply=%region_6.0 | all-reduce | flops 8448 | bytes 67584 | tf_op jit(solution)/shard_map/psum | solution.py:98
  881.6 1.9 all_gather.11
  883.5 0.7 fusion.20
  884.1 0.0 all-reduce.2.cloned.1.call-done
  884.1 2.0 fusion.18
  886.2 1.5 copy.13
  887.7 1.5 copy.14
  889.3 0.0 reduce-scatter.2.cloned.1.call-done
  (10 shorter events, 0.2 us)
Async XLA Ops:
  7.2 3.5 copy-start.3
  7.2 3.5 copy-start.4
  7.2 14.9 %all-gather.5.cloned.1.call-start = ((), (), s32[]{:S(2)}) async-start(), calls=%async_computation.3 | async-start | bytes 2359296 | tf_op jit(solution)/shard_map/all_gather | solution.py:52
  7.9 181.5 %all-gather.3.cloned.1.call-start = ((), (), s32[]{:S(2)}) async-start(), calls=%async_computation.2 | async-start | bytes 12976128 | tf_op jit(solution)/shard_map/all_gather | solution.py:61
  10.6 873.6 %all-reduce.2.cloned.1.call-start = ((), (), s32[]{:S(2)}) async-start(), calls=%async_computation.5 | async-start | bytes 5767168 | tf_op jit(solution)/shard_map/psum | solution.py:97
  22.1 173.1 %copy-start.6 = (bf16[1,384,2048]{2,1,0:T(8,128)(2,1)S(1)}, bf16[1,384,2048]{2,1,0:T(8,128)(2,1)}, u32[]{:S(2)}) copy-start(bf16[1,384,2048]{2,1,0:T(8,128)(2,1)} %all-gather.5.cloned.1.call-done) | copy-start | bytes 4718596
  189.4 6.4 copy-start.5
  198.4 5.9 collective-permute-start.1
  199.7 5.9 collective-permute-start
  206.1 1.3 copy-start.2
  208.6 5.7 collective-permute-start.3
  212.8 5.9 collective-permute-start.2
  222.9 3.2 copy-start
  790.2 5.4 copy-start.1
  790.2 99.0 %reduce-scatter.2.cloned.1.call-start = ((), (), s32[]{:S(2)}) async-start(), calls=%async_computation.4 | async-start | bytes 2359296 | tf_op jit(solution)/shard_map/reduce_scatter | solution.py:81
Sparse Core Ops, SparseCore 0:
  9.5 12.5 all-gather.4
  24.9 164.4 all-gather.2
  790.3 80.2 all-reduce.1
  873.3 8.9 reduce-scatter.1
where the time goes:
time: 897 us; the launch traced here: 896 us
  blocking collectives  583 us (65%)
  waiting for transfers between devices  185 us (21%)
  local copies, waits for them, and re-layouts  41.5 us (5%)
  other arithmetic  31.7 us (4%)
  matrix products  28.2 us (3%)
  between operations  14 us (2%)
  starting transfers between devices  11.9 us (1%)
    all_to_all x1, blocking collectives, shards(): lax.all_to_all(grad_terms, 'fs', split_axis=1, concat_axis=0, tiled=True)  504 us
    all_gather x1, waiting for transfers between devices, shards(): full_rows = lax.all_gather(stacked, 'fs', axis=1, tiled=True)  167 us
    psum x1, blocking collectives, shards(): taps_total = lax.psum(tap_terms, ('rep', 'fs'))  77.6 us
    another operation x1, local copies, waits for them, and re-layouts, shards(): jnp.stack([lax.dot_general(gathered, pre_cot[0], contract_rows, preferred...  34.1 us
  transfers between devices with their start and end apart: 8, of which 4 were waited for; matrix products, arithmetic and copies ran while one was open for 2% of the time, Pallas kernels for 0%

commit v1 on v0

v1 whole, which is shorter than its diff:
```python
import jax
import jax.numpy as jnp
from jax import lax
from jax.sharding import PartitionSpec as P

HALO = 8


def shift(x, axis, step):
    count = lax.axis_size(axis)
    return lax.ppermute(x, axis, [(i, (i + step) % count) for i in range(count)])


def with_halo(rows):
    count = lax.axis_size("fs")
    nxt = lax.ppermute(rows[:HALO], "fs", [(i + 1, i) for i in range(count - 1)])
    prv = lax.ppermute(rows[rows.shape[0] - HALO:], "fs", [(i, i + 1) for i in range(count - 1)])
    return jnp.concatenate([rows, nxt, prv], axis=0)


def before(x):
    return jnp.concatenate([x[:, -1:], x[:, :-1]], axis=1)


def after(x):
    return jnp.concatenate([x[:, 1:], x[:, :1]], axis=1)


def shards(inputs, gate_proj, value_proj, gate_taps, value_taps, out_grad):
    contract_cols = (((1,), (1,)), ((), ()))
    contract_rows = (((0,), (0,)), ((), ()))
    reps, fs_count = lax.axis_size("rep"), lax.axis_size("fs")
    rep = lax.axis_index("rep")
    tokens, feats = inputs.shape[1:]
    hid = gate_proj.shape[1]
    width = min(hid, -(-hid // reps // 128) * 128)
    last = hid - width

    def start_of(part):
        return jnp.minimum(part * width, last)

    first = start_of(rep)
    dead = rep * width - first
    live = jnp.arange(width) >= dead

    def part_cols(x, part):
        return lax.dynamic_slice_in_dim(x, start_of(part), width, x.ndim - 1)

    w_own = jnp.concatenate(
        [jnp.where(live, part_cols(w, rep), jnp.zeros((), w.dtype)) for w in (gate_proj, value_proj)], axis=1
    )
    w_all = lax.all_gather(w_own, "fs", axis=0, tiled=True)

    x_ext = with_halo(inputs[0])
    g_ext = with_halo(out_grad[0])
    x_blocks, g_blocks = [x_ext], [part_cols(g_ext, rep)]
    for step in range(1, reps):
        x_blocks.append(shift(x_ext, "rep", step))
        g_blocks.append(shift(part_cols(g_ext, (rep + step) % reps), "rep", step))
    x_all = lax.all_gather(jnp.stack(x_blocks), "tp", axis=2, tiled=True)
    g_all = jnp.stack(g_blocks).astype(jnp.float32)

    ext = tokens + 2 * HALO
    pre = jnp.dot(x_all.reshape(reps * ext, -1), w_all, preferred_element_type=jnp.float32)
    pre = pre.astype(jnp.bfloat16).astype(jnp.float32).reshape(reps, ext, 2 * width)
    tap_start = lax.axis_index("tp") * hid + first
    taps = jnp.concatenate(
        [lax.dynamic_slice_in_dim(t, tap_start, width, 1) for t in (gate_taps, value_taps)], axis=1
    )
    pre_b, pre_a = before(pre), after(pre)
    mix = taps[0] * pre_b + taps[1] * pre + taps[2] * pre_a
    gate_mix, value_mix = mix[..., :width], mix[..., width:]
    sig = jax.nn.sigmoid(gate_mix)
    gate_cot = g_all * value_mix * (sig * (1.0 + gate_mix * (1.0 - sig)))
    value_cot = g_all * (gate_mix * sig)
    cot = jnp.concatenate([gate_cot, value_cot], axis=2)
    pre_cot = taps[0] * after(cot) + taps[1] * cot + taps[2] * before(cot)
    pre_cot = pre_cot[:, :tokens].astype(jnp.bfloat16).reshape(reps * tokens, 2 * width)
    tap_terms = jnp.stack(
        [jnp.sum(p[:, :tokens] * cot[:, :tokens], axis=(0, 1)) for p in (pre_b, pre, pre_a)]
    )
    factor = float(tokens * fs_count * reps) ** (-0.5)

    grads = lax.dot_general(
        x_all[:, :tokens].reshape(reps * tokens, -1), pre_cot, contract_rows, preferred_element_type=jnp.float32
    )
    grads = (grads * factor).astype(jnp.bfloat16)
    own = lax.psum_scatter(grads, "fs", scatter_dimension=0, tiled=True)

    partial_value = lax.dot_general(pre_cot, w_all, contract_cols, preferred_element_type=jnp.float32)
    partial_value = lax.psum_scatter(
        partial_value.astype(jnp.bfloat16), "tp", scatter_dimension=1, tiled=True
    ).reshape(reps, tokens, feats)
    in_grad = partial_value[0].astype(jnp.float32)
    for step in range(1, reps):
        in_grad += shift(partial_value[step], "rep", -step).astype(jnp.float32)

    blocks = [own]
    for step in range(1, reps):
        blocks.append(shift(own, "rep", step))
    proj_grads = []
    for branch in range(2):
        cols = jnp.zeros((own.shape[0], hid), jnp.bfloat16)
        cut = [b[:, branch * width : (branch + 1) * width] for b in blocks]
        for step in range(reps):
            part = (rep - step) % reps
            place = start_of(part)
            skip = part * width - place
            old = lax.dynamic_slice_in_dim(cols, place, width, 1)
            new = jnp.where(jnp.arange(width) >= skip, cut[step], old)
            cols = lax.dynamic_update_slice_in_dim(cols, new, place, 1)
        proj_grads.append(cols.astype(jnp.float32))

    tap_sum = lax.psum(tap_terms * factor, "fs").reshape(3, 2, width)
    tap_all = lax.all_gather(lax.all_gather(tap_sum, "rep"), "tp")
    halves = []
    for half in range(tap_all.shape[0]):
        cols = [tap_all[half, p, :, :, max(0, p * width - last) if p * width > last else 0 :] for p in range(reps)]
        halves.append(jnp.concatenate(cols, axis=2))
    taps_out = jnp.concatenate(halves, axis=2)
    return in_grad.astype(jnp.bfloat16)[None], proj_grads[0], proj_grads[1], taps_out[:, 0], taps_out[:, 1]


def solution(mesh):
    placed = (P("rep", "fs", "tp"), P("fs", "tp"), P("fs", "tp"), P(), P(), P("rep", "fs", "tp"))
    return jax.shard_map(
        shards,
        mesh=mesh,
        in_specs=placed,
        out_specs=(P("rep", "fs", "tp"), P("fs", "tp"), P("fs", "tp"), P(), P()),
        check_vma=False,
    )
```

time: 897 us -> 369 us (0.41)
  blocking collectives: 583 us -> 41.8 us
  waiting for transfers between devices: 185 us -> 211 us
  local copies, waits for them, and re-layouts: 41.5 us -> 29 us
    all_to_all x1 -> x0, blocking collectives: 504 us -> none  [shards(): lax.all_to_all(grad_terms, 'fs', split_axis=1, concat_axis=0, tiled=True)]
    all_gather x2, waiting for transfers between devices: 179 us -> 97.7 us  [the longest x1 97.7 us: shards(): w_all = lax.all_gather(w_own, 'fs', axis=0, tiled=True)]
    reduce_scatter x0 -> x1, waiting for transfers between devices: none -> 78.4 us  [shards(): own = lax.psum_scatter(grads, 'fs', scatter_dimension=0, tiled=True)]
    psum x1, blocking collectives: 77.6 us -> 35.6 us  [shards(): tap_sum = lax.psum(tap_terms * factor, 'fs').reshape(3, 2, width)]
    another operation x6 -> x7, local copies, waits for them, and re-layouts: 34.1 us -> 1.73 us  [the longest x1 1.58 us: shards(): g_all = jnp.stack(g_blocks).astype(jnp.float32)]
    ppermute x4 -> x8, waiting for transfers between devices: 5.76 us -> 34.5 us  [the longest x4 19.9 us: shift(): lax.ppermute(x, axis, [(i, (i + step) % count) for i in range(count)])]
    dynamic_update_slice x0 -> x4, local copies, waits for them, and re-layouts: none -> 15 us  [shards(): cols = lax.dynamic_update_slice_in_dim(cols, new, place, 1)]
    another operation x4 -> x2, other arithmetic: 11.4 us -> 1.74 us  [shards(): x_all = lax.all_gather(jnp.stack(x_blocks), 'tp', axis=2, tiled=True)]
  transfers between devices with their start and end apart: 8 -> 12, of which waited for: 4 -> 6; matrix products, arithmetic and copies ran while one was open for 2% -> 12% of each run, Pallas kernels for 0% -> 0%
where the time goes in v1:
time: 369 us; the launch traced here: 367 us
  waiting for transfers between devices  211 us (57%)
  blocking collectives  41.8 us (11%)
  local copies, waits for them, and re-layouts  29 us (8%)
  matrix products  26.4 us (7%)
  other arithmetic  24.8 us (7%)
  starting transfers between devices  20.1 us (5%)
  between operations  14.2 us (4%)
    all_gather x1, waiting for transfers between devices, shards(): w_all = lax.all_gather(w_own, 'fs', axis=0, tiled=True)  97.7 us
    reduce_scatter x1, waiting for transfers between devices, shards(): own = lax.psum_scatter(grads, 'fs', scatter_dimension=0, tiled=True)  78.4 us
    psum x1, blocking collectives, shards(): tap_sum = lax.psum(tap_terms * factor, 'fs').reshape(3, 2, width)  35.6 us
    ppermute x4, waiting for transfers between devices, shift(): lax.ppermute(x, axis, [(i, (i + step) % count) for i in range(count)])  19.9 us
    dynamic_update_slice x4, local copies, waits for them, and re-layouts, shards(): cols = lax.dynamic_update_slice_in_dim(cols, new, place, 1)  15 us
    ppermute x2, starting transfers between devices, with_halo(): lax.ppermute(rows[rows.shape[0] - HALO:], 'fs', [(i, i + 1) for i in rang...  11.1 us
    ppermute x2, waiting for transfers between devices, with_halo(): lax.ppermute(rows[rows.shape[0] - HALO:], 'fs', [(i, i + 1) for i in rang...  9.85 us
    dot_general x1, matrix products, shards(): lax.dot_general(pre_cot, w_all, contract_cols, preferred_element_type=jnp...  9.32 us
  transfers between devices with their start and end apart: 12, of which 6 were waited for; matrix products, arithmetic and copies ran while one was open for 12% of the time, Pallas kernels for 0%

profile of v1, /device:TPU:0, one launch (start us, length us, event | category | flops | bytes accessed | tf_op | source)
XLA Modules:
  0.0 367.0 jit_solution(3353467001362223861)
XLA Ops:
  7.2 0.0 all-gather.4.cloned.1.call-start
  7.2 1.5 copy.18
  8.7 0.1 slice_bitcast_fusion.1
  8.8 4.9 %collective-permute-start.4 = (bf16[8,1024]{0,1:T(8,128)(2,1)S(1)}, bf16[8,1024]{0,1:T(8,128)(2,1)S(1)}, u32[]{:S(2)}, u32[]{:S(2)}) collective-permute-start(bf16[8,1024]{0,1:T(8,128)(2,1)S(1)} %get-tuple-element.31), channel_id=1, source_target_pairs={{0,2},{2,4},{4,6},{6,8},{8,10},{10,12},{12,14},{1,3},{3,5},{5,7},{... | collective-permute-start | bytes 49160 | tf_op jit(solution)/shard_map/ppermute | solution.py:17
  13.8 1.3 collective-permute-start.3
  15.1 9.8 %collective-permute-done.4 = bf16[8,1024]{0,1:T(8,128)(2,1)S(1)} collective-permute-done((bf16[8,1024]{0,1:T(8,128)(2,1)S(1)}, bf16[8,1024]{0,1:T(8,128)(2,1)S(1)}, u32[]{:S(2)}, u32[]{:S(2)}) %collective-permute-start.4) | collective-permute-done | bytes 16416 | tf_op jit(solution)/shard_map/ppermute | solution.py:17
  24.9 0.2 pad_maximum_fusion.7
  25.1 0.5 copy.21
  25.6 1.6 collective-permute-start.5
  27.1 0.2 fusion.33
  27.3 15.8 %collective-permute-done.5 = bf16[400,1024]{1,0:T(8,128)(2,1)} collective-permute-done((bf16[400,1024]{1,0:T(8,128)(2,1)S(1)}, bf16[400,1024]{1,0:T(8,128)(2,1)}, u32[]{:S(2)}, u32[]{:S(2)}) %collective-permute-start.5) | collective-permute-done | bytes 819232 | tf_op jit(solution)/shard_map/ppermute | solution.py:11
  43.1 1.4 copy.22
  44.6 0.0 copy-start.1
  44.6 1.6 pad_maximum_fusion.4
  46.2 0.0 all-gather.4.cloned.1.call-update
  46.2 0.0 all-gather.6.cloned.1.call-start
  46.2 1.5 dynamic-slice_select_fusion.1
  47.8 0.9 pad_maximum_fusion.8
  48.7 0.0 all-gather.6.cloned.1.call-update
  48.8 0.0 reduce-scatter.3.cloned.1.call-start
  48.8 6.2 %collective-permute-start.1 = (bf16[8,1408]{1,0:T(8,128)(2,1)S(1)}, bf16[8,1408]{1,0:T(8,128)(2,1)S(1)}, u32[]{:S(2)}, u32[]{:S(2)}) collective-permute-start(bf16[8,1408]{1,0:T(8,128)(2,1)S(1)} %get-tuple-element.25), channel_id=1, source_target_pairs={{0,2},{2,4},{4,6},{6,8},{8,10},{10,12},{12,14},{1,3},{3,5},{5,7},{... | collective-permute-start | bytes 67592 | tf_op jit(solution)/shard_map/ppermute | solution.py:17
  55.0 1.5 collective-permute-start
  56.5 0.8 constant_dynamic-slice_fusion.1
  57.3 0.1 maximum_reduce_fusion.1
  57.4 4.8 %collective-permute-done = bf16[8,1408]{1,0:T(8,128)(2,1)S(1)} collective-permute-done((bf16[8,1408]{1,0:T(8,128)(2,1)S(1)}, bf16[8,1408]{1,0:T(8,128)(2,1)S(1)}, u32[]{:S(2)}, u32[]{:S(2)}) %collective-permute-start) | collective-permute-done | bytes 22560 | tf_op jit(solution)/shard_map/ppermute | solution.py:16
  62.1 0.1 pad_maximum_fusion.6
  62.2 1.6 dynamic-slice_bitcast_fusion
  63.8 1.4 collective-permute-start.2
  65.2 4.7 %copy.23 = bf16[2,400,2048]{2,1,0:T(8,128)(2,1)S(1)} copy(bf16[2,400,2048]{1,2,0:T(8,128)(2,1)} %all-gather.4.cloned.1.call-done) | data formatting | bytes 6553600 | tf_op jit(solution)/shard_map/all_gather | solution.py:60
  69.9 97.7 %all-gather.6.cloned.1.call-done = bf16[2048,1536]{1,0:T(8,128)(2,1)} async-done(((bf16[256,1536]{1,0:T(8,128)(2,1)}), bf16[2048,1536]{1,0:T(8,128)(2,1)}) %all-gather.6.cloned.1.call-update) | async-done | bytes 6291472 | tf_op jit(solution)/shard_map/all_gather | solution.py:52
  167.6 8.2 %convolution_convert_fusion = bf16[800,1536]{1,0:T(8,128)(2,1)S(1)} fusion(bf16[800,2048]{1,0:T(8,128)(2,1)S(1)} %bitcast.55, bf16[2048,1536]{1,0:T(8,128)(2,1)} %all-gather.6.cloned.1.call-done), kind=kOutput, calls=%fused_computation.37 | convolution fusion | flops 5034393600 | bytes 12025856 | tf_op jit(solution)/shard_map/dot_general | solution.py:64
  175.8 0.7 convert.5
  176.5 1.3 fusion.24
  177.8 0.0 copy-start
  177.8 1.7 fusion.3
  179.5 2.2 convert_multiply_fusion
  181.7 1.1 fusion.4
  182.8 8.2 %fusion.15 = (f32[1536]{0:T(1024)S(1)}, f32[1536]{0:T(1024)S(1)}, f32[1536]{0:T(1024)S(1)}, bf16[2,384,1536]{2,1,0:T(8,128)(2,1)S(1)}) fusion(f32[2,400,1536]{2,1,0:T(8,128)S(1)} %convert.5, f32[2,400,768]{2,1,0:T(8,128)S(1)} %get-tuple-element.11, f32[2,400,768]{2,1,0:T(8,128)S(1)} %get-tuple-element.12, f32[2,399,1536]{2,1,0:T(8,128)S(1)} %get-tuple-element.18, ...), kind=kLoop, calls=%fused_computation.31 | loop fusion | flops 20049408 | bytes 31494144 | tf_op jit(solution)/shard_map/reduce_sum | solution.py:80
  191.1 9.3 %convolution_convert_fusion.1 = bf16[768,2048]{1,0:T(8,128)(2,1)} fusion(bf16[768,1536]{1,0:T(8,128)(2,1)S(1)} %bitcast.56, bf16[2048,1536]{1,0:T(8,128)(2,1)} %all-gather.6.cloned.1.call-done), kind=kOutput, calls=%fused_computation.38 | convolution fusion | flops 4833411072 | bytes 11796480 | tf_op jit(solution)/shard_map/dot_general | solution.py:90
  200.4 0.0 reduce-scatter.3.cloned.1.call-update
  200.4 0.3 reduce-scatter.5.cloned.1.call-start
  200.7 8.9 %fusion = bf16[2048,1536]{1,0:T(8,128)(2,1)} fusion(bf16[2,384,1536]{2,1,0:T(8,128)(2,1)S(1)} %get-tuple-element.13, bf16[2,400,2048]{1,2,0:T(8,128)(2,1)} %all-gather.4.cloned.1.call-done), kind=kOutput, calls=%fused_computation.1 | convolution fusion | flops 4838129664 | bytes 11796480 | tf_op jit(solution)/shard_map/dot_general | solution.py:84
  209.6 0.0 reduce-scatter.5.cloned.1.call-update
  209.8 35.6 %psum.7 = f32[1,3,2,768]{3,2,1,0:T(2,128)S(1)} all-reduce(f32[1,3,2,768]{3,2,1,0:T(2,128)S(1)} %all_gather_reshape.3), channel_id=1, replica_groups=mesh['rep'=2,'fs'=8,'tp'=2] {'fs'}, use_global_device_ids=true, to_apply=%region_5.6 | all-reduce | flops 4608 | bytes 36864 | tf_op jit(solution)/shard_map/psum | solution.py:114
  245.4 4.4 %all_gather.17 = f32[2,3,2,768]{3,2,1,0:T(2,128)S(1)} all-gather(f32[1,3,2,768]{3,2,1,0:T(2,128)S(1)} %psum.7), channel_id=1, replica_groups=mesh['rep'=2,'fs'=8,'tp'=2] {'rep'}, dimensions={0}, use_global_device_ids=true | all-gather | bytes 55296 | tf_op jit(solution)/shard_map/all_gather | solution.py:115
  249.8 1.8 all-gather
  251.7 0.0 reduce-scatter.3.cloned.1.call-done
  251.7 1.2 slice.184
  252.9 1.4 collective-permute-start.6
  254.3 78.4 %reduce-scatter.5.cloned.1.call-done = bf16[256,1536]{1,0:T(8,128)(2,1)} async-done(((bf16[2048,1536]{1,0:T(8,128)(2,1)}), bf16[256,1536]{1,0:T(8,128)(2,1)}) %reduce-scatter.5.cloned.1.call-update) | async-done | bytes 786448 | tf_op jit(solution)/shard_map/reduce_scatter | solution.py:88
  332.7 1.5 collective-permute-start.7
  334.2 0.6 slice_bitcast_fusion.2
  334.8 2.3 fusion.20
  337.2 1.2 slice_select_fusion.1
  338.3 0.1 broadcast.11.clone
  338.4 4.4 %dynamic_update_slice.12 = bf16[256,1408]{1,0:T(8,128)(2,1)S(1)} dynamic-update-slice(bf16[256,1408]{1,0:T(8,128)(2,1)S(1)} %broadcast.11.clone, bf16[256,768]{1,0:T(8,128)(2,1)S(1)} %get-tuple-element.29, s32[]{:T(128)} %constant.42.clone.1, s32[]{:T(128)S(6)} %select_n.69) | dynamic-update-slice | bytes 786436 | tf_op jit(solution)/shard_map/dynamic_update_slice | solution.py:111
  342.8 0.1 broadcast.11.clone.1
  342.9 4.4 %dynamic_update_slice.14 = bf16[256,1408]{1,0:T(8,128)(2,1)S(1)} dynamic-update-slice(bf16[256,1408]{1,0:T(8,128)(2,1)S(1)} %broadcast.11.clone.1, bf16[256,768]{1,0:T(8,128)(2,1)S(1)} %get-tuple-element.28, s32[]{:T(128)} %constant.42.clone.1, s32[]{:T(128)S(6)} %select_n.69) | dynamic-update-slice | bytes 786436 | tf_op jit(solution)/shard_map/dynamic_update_slice | solution.py:111
  347.3 4.1 %collective-permute-done.7 = bf16[256,1536]{1,0:T(8,128)(2,1)S(1)} collective-permute-done((bf16[256,1536]{1,0:T(8,128)(2,1)}, bf16[256,1536]{1,0:T(8,128)(2,1)S(1)}, u32[]{:S(2)}, u32[]{:S(2)}) %collective-permute-start.7) | collective-permute-done | bytes 786464 | tf_op jit(solution)/shard_map/ppermute | solution.py:11
  351.4 0.4 slice_select_fusion
  351.9 3.1 dynamic_update_slice.13
  355.0 1.2 convert_element_type.36
  356.2 3.0 dynamic_update_slice.15
  359.3 1.2 convert_element_type.37
  (25 shorter events, 0.2 us)
Async XLA Ops:
  7.2 58.1 %all-gather.4.cloned.1.call-start = ((), (), s32[]{:S(2)}) async-start(), calls=%async_computation.2 | async-start | bytes 6291456 | tf_op jit(solution)/shard_map/all_gather | solution.py:60
  8.8 16.1 %collective-permute-start.4 = (bf16[8,1024]{0,1:T(8,128)(2,1)S(1)}, bf16[8,1024]{0,1:T(8,128)(2,1)S(1)}, u32[]{:S(2)}, u32[]{:S(2)}) collective-permute-start(bf16[8,1024]{0,1:T(8,128)(2,1)S(1)} %get-tuple-element.31), channel_id=1, source_target_pairs={{0,2},{2,4},{4,6},{6,8},{8,10},{10,12},{12,14},{1,3},{3,5},{5,7},{... | collective-permute-start | bytes 49160 | tf_op jit(solution)/shard_map/ppermute | solution.py:17
  13.8 11.2 %collective-permute-start.3 = (bf16[8,1024]{0,1:T(8,128)(2,1)S(1)}, bf16[8,1024]{0,1:T(8,128)(2,1)S(1)}, u32[]{:S(2)}, u32[]{:S(2)}) collective-permute-start(bf16[8,1024]{0,1:T(8,128)(2,1)S(1)} %get-tuple-element.30), channel_id=1, source_target_pairs={{2,0},{4,2},{6,4},{8,6},{10,8},{12,10},{14,12},{3,1},{5,3},{7,5},{... | collective-permute-start | bytes 49160 | tf_op jit(solution)/shard_map/ppermute | solution.py:16
  25.6 17.5 %collective-permute-start.5 = (bf16[400,1024]{1,0:T(8,128)(2,1)S(1)}, bf16[400,1024]{1,0:T(8,128)(2,1)}, u32[]{:S(2)}, u32[]{:S(2)}) collective-permute-start(bf16[400,1024]{1,0:T(8,128)(2,1)S(1)} %copy.21), channel_id=1, source_target_pairs={{0,16},{16,0},{1,17},{17,1},{2,18},{18,2},{3,19},{19,3},{4,20},{20... | collective-permute-start | bytes 2457608 | tf_op jit(solution)/shard_map/ppermute | solution.py:11
  44.6 4.2 %copy-start.1 = (bf16[1,384,1408]{2,1,0:T(8,128)(2,1)S(1)}, bf16[1,384,1408]{2,1,0:T(8,128)(2,1)}, u32[]{:S(2)}) copy-start(bf16[1,384,1408]{2,1,0:T(8,128)(2,1)} %param.11) | copy-start | bytes 3244036
  46.2 121.4 %all-gather.6.cloned.1.call-start = ((), (), s32[]{:S(2)}) async-start(), calls=%async_computation.3 | async-start | bytes 7077888 | tf_op jit(solution)/shard_map/all_gather | solution.py:52
  48.8 203.0 %reduce-scatter.3.cloned.1.call-start = ((), (), s32[]{:S(2)}) async-start(), calls=%async_computation.4 | async-start | bytes 4718592 | tf_op jit(solution)/shard_map/reduce_scatter | solution.py:91
  48.8 8.5 %collective-permute-start.1 = (bf16[8,1408]{1,0:T(8,128)(2,1)S(1)}, bf16[8,1408]{1,0:T(8,128)(2,1)S(1)}, u32[]{:S(2)}, u32[]{:S(2)}) collective-permute-start(bf16[8,1408]{1,0:T(8,128)(2,1)S(1)} %get-tuple-element.25), channel_id=1, source_target_pairs={{0,2},{2,4},{4,6},{6,8},{8,10},{10,12},{12,14},{1,3},{3,5},{5,7},{... | collective-permute-start | bytes 67592 | tf_op jit(solution)/shard_map/ppermute | solution.py:17
  55.0 7.1 %collective-permute-start = (bf16[8,1408]{1,0:T(8,128)(2,1)S(1)}, bf16[8,1408]{1,0:T(8,128)(2,1)S(1)}, u32[]{:S(2)}, u32[]{:S(2)}) collective-permute-start(bf16[8,1408]{1,0:T(8,128)(2,1)S(1)} %get-tuple-element.24), channel_id=1, source_target_pairs={{2,0},{4,2},{6,4},{8,6},{10,8},{12,10},{14,12},{3,1},{5,3},{7,5},{... | collective-permute-start | bytes 67592 | tf_op jit(solution)/shard_map/ppermute | solution.py:16
  63.8 115.7 %collective-permute-start.2 = (bf16[400,768]{1,0:T(8,128)(2,1)}, bf16[400,768]{1,0:T(8,128)(2,1)}, u32[]{:S(2)}, u32[]{:S(2)}) collective-permute-start(bf16[400,768]{1,0:T(8,128)(2,1)} %get-tuple-element.23), channel_id=1, source_target_pairs={{0,16},{16,0},{1,17},{17,1},{2,18},{18,2},{3,19},{19,3},{4,20},{20... | collective-permute-start | bytes 1843208 | tf_op jit(solution)/shard_map/ppermute | solution.py:11
  177.8 1.7 copy-start
  200.4 132.3 %reduce-scatter.5.cloned.1.call-start = ((), (), s32[]{:S(2)}) async-start(), calls=%async_computation.5 | async-start | bytes 7077888 | tf_op jit(solution)/shard_map/reduce_scatter | solution.py:88
  252.9 81.9 %collective-permute-start.6 = (bf16[384,1024]{1,0:T(8,128)(2,1)S(1)}, bf16[384,1024]{1,0:T(8,128)(2,1)S(1)}, u32[]{:S(2)}, u32[]{:S(2)}) collective-permute-start(bf16[384,1024]{1,0:T(8,128)(2,1)S(1)} %slice.184), channel_id=1, source_target_pairs={{0,16},{16,0},{1,17},{17,1},{2,18},{18,2},{3,19},{19,3},{4,20},{20... | collective-permute-start | bytes 2359304 | tf_op jit(solution)/shard_map/ppermute | solution.py:11
  332.7 18.7 %collective-permute-start.7 = (bf16[256,1536]{1,0:T(8,128)(2,1)}, bf16[256,1536]{1,0:T(8,128)(2,1)S(1)}, u32[]{:S(2)}, u32[]{:S(2)}) collective-permute-start(bf16[256,1536]{1,0:T(8,128)(2,1)} %reduce-scatter.5.cloned.1.call-done), channel_id=1, source_target_pairs={{0,16},{16,0},{1,17},{17,1},{2,18},{18,2},{3,19},{19,3},{4,20},{20... | collective-permute-start | bytes 2359304 | tf_op jit(solution)/shard_map/ppermute | solution.py:11
Sparse Core Ops, SparseCore 0:
  46.3 18.6 all-gather.3
  67.7 99.8 all-gather.5
  200.5 9.1 reduce-scatter.2
  213.1 119.5 reduce-scatter.4
